TPU v7x, 32 devices: a whole 2x2x4 slice. The times are simulated.
32 devices in a mesh: fs: 4 (over y, x), tp: 8 (over z, core).
Axes of the slice: x: 2, y: 2, z: 4, core: 2. Of those that a mesh axis runs over, the one named last changes fastest.
Arguments:
- normed_inputs: bfloat16 [4096, 4096], P('fs', 'tp'), may hold values from -6 to 6
- query_upstream: bfloat16 [4096, 4096], P('fs', 'tp'), may hold values from -0.125 to 0.125
- key_upstream: bfloat16 [4096, 1024], P('fs', 'tp'), may hold values from -0.09375 to 0.09375
- head_outputs: bfloat16 [4096, 4096], P('fs', 'tp'), may hold values from -6 to 6
- branch_upstream: bfloat16 [4096, 4096], P('fs', 'tp'), may hold values from -0.125 to 0.125
- query_master: float32 [4096, 4096], P('fs', 'tp'), may hold values from -0.09375 to 0.09375
- key_master: float32 [4096, 1024], P('fs', 'tp'), may hold values from -0.09375 to 0.09375
- branch_master: float32 [4096, 4096], P('fs', 'tp'), may hold values from -0.09375 to 0.09375
- query_basis: bfloat16 [4096, 128], replicated, may hold values from -0.09375 to 0.09375
- key_basis: bfloat16 [4096, 128], replicated, may hold values from -0.09375 to 0.09375
- branch_basis: bfloat16 [4096, 128], replicated, may hold values from -0.09375 to 0.09375
- query_first: float32 [128, 4096], P(None, 'tp'), may hold values from -0.75 to 0.75
- query_second: float32 [128, 4096], P(None, 'tp'), may hold values from 0.001 to 0.02
- key_first: float32 [128, 1024], P(None, 'tp'), may hold values from -0.75 to 0.75
- key_second: float32 [128, 1024], P(None, 'tp'), may hold values from 0.001 to 0.02
- branch_first: float32 [4096, 128], P('fs'), may hold values from -0.75 to 0.75
- branch_second: float32 [4096, 128], P('fs'), may hold values from 0.001 to 0.02
Outputs:
- query_step: float32 [4096, 4096], P('fs', 'tp')
- key_step: float32 [4096, 1024], P('fs', 'tp')
- branch_step: float32 [4096, 4096], P('fs', 'tp')
- query_updated: float32 [4096, 4096], P('fs', 'tp')
- key_updated: float32 [4096, 1024], P('fs', 'tp')
- branch_updated: float32 [4096, 4096], P('fs', 'tp')
- query_copy: bfloat16 [4096, 4096], P(None, 'tp')
- key_copy: bfloat16 [4096, 1024], P(None, 'tp')
- branch_copy: bfloat16 [4096, 4096], P(None, 'tp')
- query_first_new: float32 [128, 4096], P(None, 'tp')
- query_second_new: float32 [128, 4096], P(None, 'tp')
- key_first_new: float32 [128, 1024], P(None, 'tp')
- key_second_new: float32 [128, 1024], P(None, 'tp')
- branch_first_new: float32 [4096, 128], P('fs')
- branch_second_new: float32 [4096, 128], P('fs')
All inputs are finite; a program needn't handle non-finite values.
Results may differ from a plain program's by a relative error of at most 0.001.
Values may be sent and summed in bfloat16 or wider, within the bound.
No kernel may reach another device: no remote copies, remote signals or barrier semaphores. Data moves between devices by JAX's collectives and lax.ppermute only.
A program may use at most 128 MiB of HBM per device.

v0:
```python
import jax
import jax.numpy as jnp
from jax import lax
from jax.sharding import PartitionSpec as P

LEARN = 0.02
BETA_ONE = 0.9
BETA_TWO = 0.95
ADAM_EPS = 1e-08
CLIP_RMS = 0.5


def moments(first, second, low, clip):
    scaled = clip * low
    first_new = BETA_ONE * first + (1.0 - BETA_ONE) * scaled
    second_new = BETA_TWO * second + (1.0 - BETA_TWO) * scaled * scaled
    return (first_new, second_new, first_new / (jnp.sqrt(second_new) + ADAM_EPS))


def over_tokens(left, right, precision=None):
    return lax.dot_general(
        left,
        right,
        (((0,), (0,)), ((), ())),
        precision=precision,
        preferred_element_type=jnp.float32,
    )


def per_device(
    normed_inputs,
    query_upstream,
    key_upstream,
    head_outputs,
    branch_upstream,
    query_master,
    key_master,
    branch_master,
    query_basis,
    key_basis,
    branch_basis,
    query_first,
    query_second,
    key_first,
    key_second,
    branch_first,
    branch_second,
):
    exact = lax.Precision.HIGHEST
    row_index = lax.axis_index("fs")
    col_index = lax.axis_index("tp")
    n_rows = lax.axis_size("fs")
    n_cols = lax.axis_size("tp")
    features = normed_inputs.shape[1]
    query_local = query_upstream.shape[1]
    key_local = key_upstream.shape[1]
    rows_in = query_master.shape[0]
    rank = query_basis.shape[1]
    whole_values = lax.all_gather(head_outputs, "tp", axis=1, tiled=True)
    block_query = lax.dynamic_slice_in_dim(query_basis, col_index * features, features, 0)
    block_key = lax.dynamic_slice_in_dim(key_basis, col_index * features, features, 0)
    proj_query, proj_key = lax.psum(
        (
            jnp.dot(normed_inputs, block_query, preferred_element_type=jnp.float32),
            jnp.dot(normed_inputs, block_key, preferred_element_type=jnp.float32),
        ),
        "tp",
    )
    part_query = over_tokens(proj_query, query_upstream.astype(jnp.float32), exact)
    part_key = over_tokens(proj_key, key_upstream.astype(jnp.float32), exact)
    grad_branch = lax.psum_scatter(
        over_tokens(whole_values, branch_upstream), "fs", scatter_dimension=0, tiled=True
    )
    own_branch = lax.dynamic_slice_in_dim(branch_basis, col_index * features, features, 0).astype(
        jnp.float32
    )
    part_branch = jnp.dot(grad_branch, own_branch, precision=exact)
    query_low, key_low = lax.psum((part_query, part_key), "fs")
    branch_low = lax.psum(part_branch, "tp")
    local_squares = (jnp.sum(query_low * query_low) + jnp.sum(key_low * key_low)) / n_rows
    local_squares = local_squares + jnp.sum(branch_low * branch_low) / n_cols
    total = lax.psum(local_squares, ("fs", "tp"))
    entries = rank * n_cols * (2 * query_local + key_local)
    rms_value = jnp.sqrt(total / float(entries))
    clip = 1.0 / jnp.maximum(1.0, rms_value / CLIP_RMS)
    q_first, q_second, q_dir = moments(query_first, query_second, query_low, clip)
    k_first, k_second, k_dir = moments(key_first, key_second, key_low, clip)
    b_first, b_second, b_dir = moments(branch_first, branch_second, branch_low, clip)
    step_rows_query = lax.dynamic_slice_in_dim(query_basis, row_index * rows_in, rows_in, 0).astype(
        jnp.float32
    )
    step_rows_key = lax.dynamic_slice_in_dim(key_basis, row_index * rows_in, rows_in, 0).astype(
        jnp.float32
    )
    query_step = jnp.dot(step_rows_query, q_dir, precision=exact)
    key_step = jnp.dot(step_rows_key, k_dir, precision=exact)
    branch_step = jnp.dot(b_dir, own_branch.T, precision=exact)
    query_updated = query_master - LEARN * query_step
    key_updated = key_master - LEARN * key_step
    branch_updated = branch_master - LEARN * branch_step
    query_copy, key_copy, branch_copy = (
        lax.all_gather(query_updated.astype(jnp.bfloat16), "fs", axis=0, tiled=True),
        lax.all_gather(key_updated.astype(jnp.bfloat16), "fs", axis=0, tiled=True),
        lax.all_gather(branch_updated.astype(jnp.bfloat16), "fs", axis=0, tiled=True),
    )
    return (
        query_step,
        key_step,
        branch_step,
        query_updated,
        key_updated,
        branch_updated,
        query_copy,
        key_copy,
        branch_copy,
        q_first,
        q_second,
        k_first,
        k_second,
        b_first,
        b_second,
    )


def solution(mesh):
    return jax.shard_map(
        per_device,
        mesh=mesh,
        in_specs=(
            P("fs", "tp"),
            P("fs", "tp"),
            P("fs", "tp"),
            P("fs", "tp"),
            P("fs", "tp"),
            P("fs", "tp"),
            P("fs", "tp"),
            P("fs", "tp"),
            P(),
            P(),
            P(),
            P(None, "tp"),
            P(None, "tp"),
            P(None, "tp"),
            P(None, "tp"),
            P("fs", None),
            P("fs", None),
        ),
        out_specs=(
            P("fs", "tp"),
            P("fs", "tp"),
            P("fs", "tp"),
            P("fs", "tp"),
            P("fs", "tp"),
            P("fs", "tp"),
            P(None, "tp"),
            P(None, "tp"),
            P(None, "tp"),
            P(None, "tp"),
            P(None, "tp"),
            P(None, "tp"),
            P(None, "tp"),
            P("fs", None),
            P("fs", None),
        ),
        check_vma=False,
    )
```

profile of v0, /device:TPU:0, one launch (start us, length us, event | category | flops | bytes accessed | tf_op | source)
XLA Modules:
  0.0 502.3 jit_solution(1356573704103843505)
XLA Ops:
  8.0 86.4 %all-gather.5.cloned.1.call-done = bf16[1024,4096]{1,0:T(8,128)(2,1)} async-done(((bf16[1024,512]{1,0:T(8,128)(2,1)}), bf16[1024,4096]{1,0:T(8,128)(2,1)}) %all-gather.5.cloned.1.call-update) | async-done | bytes 8388624 | tf_op jit(solution)/shard_map/all_gather | solution.py:59
  94.4 10.4 %fusion.39 = f32[4096,512]{1,0:T(8,128)} fusion(bf16[1024,4096]{1,0:T(8,128)(2,1)} %all-gather.5.cloned.1.call-done, bf16[1024,512]{1,0:T(8,128)(2,1)S(1)} %copy-done), kind=kOutput, calls=%fused_computation.53 | convolution fusion | flops 4294967296 | bytes 17825792 | tf_op jit(solution)/shard_map/dot_general | solution.py:21
  104.9 1.1 copy-done.2
  106.1 2.2 convolution_bitcast_fusion
  108.2 2.2 convolution_bitcast_fusion.1
  110.4 79.4 %reduce-scatter.2.cloned.1.call-done = f32[1024,512]{1,0:T(8,128)} async-done(((f32[4096,512]{1,0:T(8,128)}), f32[1024,512]{1,0:T(8,128)}) %reduce-scatter.2.cloned.1.call-update) | async-done | bytes 2097168 | tf_op jit(solution)/shard_map/reduce_scatter | solution.py:71
  189.8 3.4 fusion.18
  193.4 62.4 %all-reduce.5.cloned.1.call-done = (f32[1024,128]{0,1:T(8,128)}, f32[1024,128]{0,1:T(8,128)}, f32[1024,128]{1,0:T(8,128)}) async-done(((f32[1024,128]{0,1:T(8,128)}, f32[1024,128]{0,1:T(8,128)}, f32[1024,128]{1,0:T(8,128)}), (f32[1024,128]{0,1:T(8,128)}, f32[1024,128]{0,1:T(8,128)}, f32[1024,128]{1,0:T(8,128)})) %all-reduce.5.cloned.1.call-update) | async-done | bytes 1572880 | tf_op jit(solution)/shard_map/psum | solution.py:62
  255.8 2.5 fusion.37
  258.3 1.0 fusion.38
  260.7 41.6 %all-reduce.7.cloned.1.call-done = (f32[128,512]{1,0:T(8,128)}, f32[128,128]{1,0:T(8,128)}) async-done(((f32[128,512]{1,0:T(8,128)}, f32[128,128]{1,0:T(8,128)}), (f32[128,512]{1,0:T(8,128)}, f32[128,128]{1,0:T(8,128)})) %all-reduce.7.cloned.1.call-update) | async-done | bytes 327696 | tf_op jit(solution)/shard_map/psum | solution.py:78
  302.3 1.6 multiply_reduce_fusion.1
  303.9 1.5 multiply_reduce_fusion.2
  306.7 39.3 %psum.47 = f32[]{:T(128)} all-reduce(f32[]{:T(128)S(6)} %add.68), channel_id=1, replica_groups=mesh['fs'=4,'tp'=8] {'fs','tp'}, use_global_device_ids=true, to_apply=%region_9.0 | all-reduce | flops 1 | bytes 8 | tf_op jit(solution)/shard_map/psum | solution.py:82
  347.7 2.6 fusion.35
  350.3 1.4 fusion
  351.7 4.7 fusion.34
  356.5 1.2 fusion.5
  358.1 4.5 fusion.36
  362.7 15.2 %all-gather.9.cloned.1.call-done = bf16[4096,128]{1,0:T(8,128)(2,1)} async-done(((bf16[1024,128]{1,0:T(8,128)(2,1)}), bf16[4096,128]{1,0:T(8,128)(2,1)}) %all-gather.9.cloned.1.call-update) | async-done | bytes 1048592 | tf_op jit(solution)/shard_map/all_gather | solution.py:103
  377.9 54.9 %all-gather.11.cloned.1.call-done = bf16[4096,512]{1,0:T(8,128)(2,1)} async-done(((bf16[1024,512]{1,0:T(8,128)(2,1)}), bf16[4096,512]{1,0:T(8,128)(2,1)}) %all-gather.11.cloned.1.call-update) | async-done | bytes 4194320 | tf_op jit(solution)/shard_map/all_gather | solution.py:104
  432.8 55.0 %all-gather.7.cloned.1.call-done = bf16[4096,512]{1,0:T(8,128)(2,1)} async-done(((bf16[1024,512]{1,0:T(8,128)(2,1)}), bf16[4096,512]{1,0:T(8,128)(2,1)}) %all-gather.7.cloned.1.call-update) | async-done | bytes 4194320 | tf_op jit(solution)/shard_map/all_gather | solution.py:102
  487.8 4.6 copy.40
  493.4 2.0 copy.42
  (60 shorter events, 4.2 us)
Async XLA Ops:
  7.2 87.2 %copy-start = (bf16[1024,512]{1,0:T(8,128)(2,1)S(1)}, bf16[1024,512]{1,0:T(8,128)(2,1)}, u32[]{:S(2)}) copy-start(bf16[1024,512]{1,0:T(8,128)(2,1)} %param.21) | copy-start | bytes 3145732
  7.2 87.2 %all-gather.5.cloned.1.call-start = ((), (), s32[]{:S(2)}) async-start(), calls=%async_computation.1 | async-start | bytes 9437184 | tf_op jit(solution)/shard_map/all_gather | solution.py:59
  7.9 181.9 %reduce-scatter.2.cloned.1.call-start = ((), (), s32[]{:S(2)}) async-start(), calls=%async_computation.2 | async-start | bytes 10485760 | tf_op jit(solution)/shard_map/reduce_scatter | solution.py:71
  104.9 150.9 %all-reduce.5.cloned.1.call-start = ((), (), s32[]{:S(2)}) async-start(), calls=%async_computation.6 | async-start | bytes 3145728 | tf_op jit(solution)/shard_map/psum | solution.py:62
  110.4 145.4 %copy-start.11 = (bf16[1024,512]{1,0:T(8,128)(2,1)S(1)}, bf16[1024,512]{1,0:T(8,128)(2,1)}, u32[]{:S(2)}) copy-start(bf16[1024,512]{1,0:T(8,128)(2,1)} %param.18) | copy-start | bytes 3145732
  193.3 65.0 %copy-start.19 = (bf16[1024,128]{1,0:T(8,128)(2,1)S(1)}, bf16[1024,128]{1,0:T(8,128)(2,1)}, u32[]{:S(2)}) copy-start(bf16[1024,128]{1,0:T(8,128)(2,1)} %param.19) | copy-start | bytes 786436
  193.3 153.5 %copy-start.20 = (f32[128,128]{1,0:T(8,128)S(1)}, f32[128,128]{1,0:T(8,128)}, u32[]{:S(2)}) copy-start(f32[128,128]{1,0:T(8,128)} %param.31) | copy-start | bytes 196612
  193.3 153.5 %copy-start.21 = (f32[128,128]{1,0:T(8,128)S(1)}, f32[128,128]{1,0:T(8,128)}, u32[]{:S(2)}) copy-start(f32[128,128]{1,0:T(8,128)} %param.30) | copy-start | bytes 196612
  193.3 109.0 %all-reduce.7.cloned.1.call-start = ((), (), s32[]{:S(2)}) async-start(), calls=%async_computation.7 | async-start | bytes 655360 | tf_op jit(solution)/shard_map/psum | solution.py:78
  255.8 91.9 %copy-start.14 = (f32[1024,128]{1,0:T(8,128)S(1)}, f32[1024,128]{1,0:T(8,128)}, u32[]{:S(2)}) copy-start(f32[1024,128]{1,0:T(8,128)} %param.23) | copy-start | bytes 1572868
  259.3 118.6 %all-gather.9.cloned.1.call-start = ((), (), s32[]{:S(2)}) async-start(), calls=%async_computation.4 | async-start | bytes 1310720 | tf_op jit(solution)/shard_map/all_gather | solution.py:103
  347.6 4.0 copy-start.17
  347.6 4.0 copy-start.18
  347.7 4.0 copy-start.7
  350.3 82.5 %all-gather.11.cloned.1.call-start = ((), (), s32[]{:S(2)}) async-start(), calls=%async_computation.5 | async-start | bytes 5242880 | tf_op jit(solution)/shard_map/all_gather | solution.py:104
  351.7 4.7 copy-start.4
  351.7 4.7 copy-start.5
  351.7 4.8 copy-start.12
  351.7 4.8 copy-start.16
  356.4 131.4 %all-gather.7.cloned.1.call-start = ((), (), s32[]{:S(2)}) async-start(), calls=%async_computation.3 | async-start | bytes 5242880 | tf_op jit(solution)/shard_map/all_gather | solution.py:102
  357.7 5.0 copy-start.9
  357.7 5.0 copy-start.10
  487.8 4.6 copy-start.13
  487.8 5.6 %copy-start.3 = (bf16[4096,512]{1,0:T(8,128)(2,1)S(1)}, bf16[4096,512]{1,0:T(8,128)(2,1)}, u32[]{:S(2)}) copy-start(bf16[4096,512]{1,0:T(8,128)(2,1)} %all-gather.11.cloned.1.call-done) | copy-start | bytes 12582916
  (5 other events, 11.0 us)
Sparse Core Ops, SparseCore 0:
  9.6 84.7 all-gather.4
  105.0 84.7 reduce-scatter.1
  193.6 62.1 all-reduce.4
  259.4 42.8 all-reduce.6
  350.4 27.4 all-gather.8
  380.2 52.5 all-gather.10
  435.2 52.5 all-gather.6
where the time goes:
time: 503 us; the launch traced here: 502 us
  waiting for transfers between devices  396 us (79%)
  blocking collectives  39.3 us (8%)
  matrix products  33.4 us (7%)
  between operations  17 us (3%)
  local copies, waits for them, and re-layouts  9.28 us (2%)
  other arithmetic  7.2 us (1%)
    all_gather x1, waiting for transfers between devices, per_device(): whole_values = lax.all_gather(head_outputs, 'tp', axis=1, tiled=True)  86.4 us
    reduce_scatter x1, waiting for transfers between devices, per_device(): lax.psum_scatter(over_tokens(whole_values, branch_upstream), 'fs', scatte...  79.4 us
    psum x1, waiting for transfers between devices, per_device(): lax.psum((jnp.dot(normed_inputs, block_query, preferred_element_type=jnp....  62.4 us
    all_gather x1, waiting for transfers between devices, per_device(): lax.all_gather(query_updated.astype(jnp.bfloat16), 'fs', axis=0, tiled=True)  55 us
    all_gather x1, waiting for transfers between devices, per_device(): lax.all_gather(branch_updated.astype(jnp.bfloat16), 'fs', axis=0, tiled=T...  54.9 us
    psum x1, waiting for transfers between devices, per_device(): query_low, key_low = lax.psum((part_query, part_key), 'fs')  41.6 us
    psum x1, blocking collectives, per_device(): total = lax.psum(local_squares, ('fs', 'tp'))  39.3 us
    all_gather x1, waiting for transfers between devices, per_device(): lax.all_gather(key_updated.astype(jnp.bfloat16), 'fs', axis=0, tiled=True)  15.2 us
  transfers between devices with their start and end apart: 7, of which 7 were waited for; matrix products, arithmetic and copies ran while one was open for 3% of the time, Pallas kernels for 0%

commit v1 on v0

v1 whole, which is shorter than its diff:
```python
import jax
import jax.numpy as jnp
from jax import lax
from jax.sharding import PartitionSpec as P

LEARN = 0.02
BETA_ONE = 0.9
BETA_TWO = 0.95
ADAM_EPS = 1e-08
CLIP_RMS = 0.5
PREFETCH = False


def moments(first, second, low, clip):
    scaled = clip * low
    first_new = BETA_ONE * first + (1.0 - BETA_ONE) * scaled
    second_new = BETA_TWO * second + (1.0 - BETA_TWO) * scaled * scaled
    return (first_new, second_new, first_new / (jnp.sqrt(second_new) + ADAM_EPS))


def over_tokens(left, right):
    return lax.dot_general(
        left, right, (((0,), (0,)), ((), ())), preferred_element_type=jnp.float32
    )


def two_terms(value):
    high = lax.reduce_precision(value, 8, 7)
    return high.astype(jnp.bfloat16), (value - high).astype(jnp.bfloat16)


def shift_pairs(groups, inner, step):
    return [
        (g * inner + i, ((g + step) % groups) * inner + i)
        for g in range(groups)
        for i in range(inner)
    ]


def xor_pairs(size, bit):
    return [(i, i ^ bit) for i in range(size)]


def piece(value, index, count):
    rows = value.shape[0] // count
    return lax.dynamic_slice_in_dim(value, index * rows, rows, 0)


def put(target, value, index):
    return lax.dynamic_update_slice_in_dim(target, value, index * value.shape[0], 0)


def sum_over(value, axis):
    size = lax.axis_size(axis)
    inner = 2 if size % 2 == 0 else 1
    groups = size // inner
    if value.shape[0] % (size * 8):
        return lax.psum(value, axis)
    spot = lax.axis_index(axis)
    own_group, own_inner = spot // inner, spot % inner
    half = value
    if inner == 2:
        got = lax.ppermute(piece(value, 1 - own_inner, 2), axis, xor_pairs(size, 1))
        half = piece(value, own_inner, 2) + got
    parts = [
        lax.ppermute(
            piece(half, (own_group + step) % groups, groups), axis, shift_pairs(groups, inner, step)
        )
        for step in range(1, groups)
    ]
    total = piece(half, own_group, groups)
    for part in parts:
        total = total + part
    others = [
        lax.ppermute(total, axis, shift_pairs(groups, inner, step)) for step in range(1, groups)
    ]
    half = put(jnp.zeros_like(half), total, own_group)
    for step, other in enumerate(others, 1):
        half = put(half, other, (own_group - step) % groups)
    if inner == 1:
        return half
    got = lax.ppermute(half, axis, xor_pairs(size, 1))
    first = own_inner == 0
    return jnp.concatenate([jnp.where(first, half, got), jnp.where(first, got, half)], axis=0)


def bits_of(size):
    return [1 << k for k in range(size.bit_length() - 1)]


def orders_of(size):
    bits = bits_of(size)
    turn = len(bits) // 2
    return bits, bits[turn:] + bits[:turn]


def doubling_sum(values, axis, orders):
    size = lax.axis_size(axis)
    if size & (size - 1):
        return [lax.psum(value, axis) for value in values]
    values = list(values)
    for stage in range(len(orders[0])):
        got = [
            lax.ppermute(value, axis, xor_pairs(size, order[stage]))
            for value, order in zip(values, orders)
        ]
        values = [value + other for value, other in zip(values, got)]
    return values


def spread_rows(value, axis):
    size = lax.axis_size(axis)
    if size & (size - 1) or value.shape[0] % 32:
        return lax.all_gather(value, axis, axis=0, tiled=True)
    rows = value.shape[0]
    half = rows // 2
    spot = lax.axis_index(axis)
    out = jnp.zeros((size * rows,) + value.shape[1:], value.dtype)
    held = [[(0, value[:half])], [(0, value[half:])]]
    for stage in range(len(bits_of(size))):
        for part, order in enumerate(orders_of(size)):
            bit = order[stage]
            held[part] += [
                (mark ^ bit, lax.ppermute(block, axis, xor_pairs(size, bit)))
                for mark, block in held[part]
            ]
    for part in range(2):
        for mark, block in held[part]:
            out = lax.dynamic_update_slice_in_dim(
                out, block, (spot ^ mark) * rows + part * half, 0
            )
    return out


def take_rows(mine, row_index, col_index, rows_in):
    n_rows, n_cols = lax.axis_size("fs"), lax.axis_size("tp")
    rows = mine.shape[0]
    count = rows_in // rows if rows_in % rows == 0 else 0
    inner = 2 if n_cols % 2 == 0 else 1
    groups = n_cols // inner
    if count == 0 or inner % count or n_rows * count != n_cols:
        whole = lax.all_gather(mine, "tp", axis=0, tiled=True)
        return lax.dynamic_slice_in_dim(whole, row_index * rows_in, rows_in, 0)

    def index(r, c):
        return r * n_cols + c

    got = mine
    own_group = col_index // inner
    for step in range(1, groups):
        pairs = []
        for r in range(n_rows):
            for c in range(r * count, (r + 1) * count):
                g, i = c // inner, c % inner
                pairs.append((index(r, c), index(r, ((g + step) % groups) * inner + i)))
        came = lax.ppermute(mine, ("fs", "tp"), pairs)
        from_group = (row_index * count) // inner
        got = jnp.where((own_group - from_group) % groups == step, came, got)
    if inner == 1:
        return got
    other = lax.ppermute(got, "tp", xor_pairs(n_cols, 1))
    first = col_index % 2 == 0
    even, odd = jnp.where(first, got, other), jnp.where(first, other, got)
    if count == 2:
        return jnp.concatenate([even, odd], axis=0)
    return jnp.where((row_index * count) % 2 == 0, even, odd)


def per_device(
    normed_inputs,
    query_upstream,
    key_upstream,
    head_outputs,
    branch_upstream,
    query_master,
    key_master,
    branch_master,
    query_basis,
    key_basis,
    branch_basis,
    query_first,
    query_second,
    key_first,
    key_second,
    branch_first,
    branch_second,
):
    row_index = lax.axis_index("fs")
    col_index = lax.axis_index("tp")
    n_rows = lax.axis_size("fs")
    n_cols = lax.axis_size("tp")
    features = normed_inputs.shape[1]
    query_local = query_upstream.shape[1]
    key_local = key_upstream.shape[1]
    rows_in = query_master.shape[0]
    rank = query_basis.shape[1]

    def own(basis):
        return lax.dynamic_slice_in_dim(basis, col_index * features, features, 0)

    own_branch = own(branch_basis)
    both = jnp.concatenate([own(query_basis), own(key_basis)], axis=1)
    proj_local = jnp.concatenate(
        [
            jnp.dot(normed_inputs, both, preferred_element_type=jnp.float32),
            jnp.dot(branch_upstream, own_branch, preferred_element_type=jnp.float32),
        ],
        axis=1,
    )
    proj = sum_over(proj_local, "tp")
    terms = [
        jnp.concatenate(two_terms(proj[:, k * rank : (k + 1) * rank]), axis=1) for k in range(3)
    ]
    part_query = over_tokens(terms[0], query_upstream)
    part_key = over_tokens(terms[1], key_upstream)
    part_branch = over_tokens(head_outputs, terms[2])
    part_query = part_query[:rank] + part_query[rank:]
    part_key = part_key[:rank] + part_key[rank:]
    part_branch = part_branch[:, :rank] + part_branch[:, rank:]
    ways = orders_of(n_rows)
    if PREFETCH:
        all_query = lax.all_gather(query_master, "fs", axis=0, tiled=True)
        all_key = lax.all_gather(key_master, "fs", axis=0, tiled=True)
    query_low, branch_mine, key_low = doubling_sum(
        (part_query, part_branch, part_key), "fs", (ways[0], ways[1], ways[0])
    )
    squares = (
        jnp.sum(query_low * query_low)
        + jnp.sum(key_low * key_low)
        + jnp.sum(branch_mine * branch_mine)
    )
    squares = jnp.full((8, 128), squares, jnp.float32)
    bits = bits_of(n_cols)
    (squares,) = doubling_sum((squares,), "tp", (bits,))
    total = squares[0, 0]
    branch_low = take_rows(branch_mine, row_index, col_index, rows_in)
    entries = rank * n_cols * (2 * query_local + key_local)
    rms_value = jnp.sqrt(total / float(entries))
    clip = 1.0 / jnp.maximum(1.0, rms_value / CLIP_RMS)
    b_first, b_second, b_dir = moments(branch_first, branch_second, branch_low, clip)
    q_first, q_second, q_dir = moments(query_first, query_second, query_low, clip)
    k_first, k_second, k_dir = moments(key_first, key_second, key_low, clip)
    branch_step = lax.dot_general(
        jnp.concatenate(two_terms(b_dir), axis=1),
        jnp.concatenate([own_branch, own_branch], axis=1),
        (((1,), (1,)), ((), ())),
        preferred_element_type=jnp.float32,
    )
    branch_updated = branch_master - LEARN * branch_step
    branch_copy = spread_rows(branch_updated.astype(jnp.bfloat16), "fs")

    def step_of(basis, direction):
        return jnp.dot(
            jnp.concatenate([basis, basis], axis=1),
            jnp.concatenate(two_terms(direction), axis=0),
            preferred_element_type=jnp.float32,
        )

    def rows_of(basis):
        return lax.dynamic_slice_in_dim(basis, row_index * rows_in, rows_in, 0)

    query_step = step_of(rows_of(query_basis), q_dir)
    key_step = step_of(rows_of(key_basis), k_dir)
    query_updated = query_master - LEARN * query_step
    key_updated = key_master - LEARN * key_step
    if PREFETCH:
        query_copy = (all_query - LEARN * step_of(query_basis, q_dir)).astype(jnp.bfloat16)
        key_copy = (all_key - LEARN * step_of(key_basis, k_dir)).astype(jnp.bfloat16)
    else:
        query_copy = spread_rows(query_updated.astype(jnp.bfloat16), "fs")
        key_copy = spread_rows(key_updated.astype(jnp.bfloat16), "fs")
    return (
        query_step,
        key_step,
        branch_step,
        query_updated,
        key_updated,
        branch_updated,
        query_copy,
        key_copy,
        branch_copy,
        q_first,
        q_second,
        k_first,
        k_second,
        b_first,
        b_second,
    )


def solution(mesh):
    return jax.shard_map(
        per_device,
        mesh=mesh,
        in_specs=(
            P("fs", "tp"),
            P("fs", "tp"),
            P("fs", "tp"),
            P("fs", "tp"),
            P("fs", "tp"),
            P("fs", "tp"),
            P("fs", "tp"),
            P("fs", "tp"),
            P(),
            P(),
            P(),
            P(None, "tp"),
            P(None, "tp"),
            P(None, "tp"),
            P(None, "tp"),
            P("fs", None),
            P("fs", None),
        ),
        out_specs=(
            P("fs", "tp"),
            P("fs", "tp"),
            P("fs", "tp"),
            P("fs", "tp"),
            P("fs", "tp"),
            P("fs", "tp"),
            P(None, "tp"),
            P(None, "tp"),
            P(None, "tp"),
            P(None, "tp"),
            P(None, "tp"),
            P(None, "tp"),
            P(None, "tp"),
            P("fs", None),
            P("fs", None),
        ),
        check_vma=False,
    )
```

time: 503 us -> 201 us (0.40)
  waiting for transfers between devices: 396 us -> 83.5 us
  starting transfers between devices: 0.28 us -> 52.1 us
  blocking collectives: 39.3 us -> 0 us
  local copies, waits for them, and re-layouts: 9.28 us -> 41.6 us
  matrix products: 33.4 us -> 10.7 us
  between operations: 17 us -> 3.97 us
    all_gather x4 -> x0, waiting for transfers between devices: 212 us -> none  [the longest x1 86.4 us: per_device(): whole_values = lax.all_gather(head_outputs, 'tp', axis=1, tiled=True)]
    psum x2 -> x0, waiting for transfers between devices: 104 us -> none  [the longest x1 62.4 us: per_device(): lax.psum((jnp.dot(normed_inputs, block_query, preferred_element_type=jnp....]
    ppermute x0 -> x39, waiting for transfers between devices: none -> 83.5 us  [the longest x18 40.1 us: spread_rows(): lax.ppermute(block, axis, xor_pairs(size, bit))]
    reduce_scatter x1 -> x0, waiting for transfers between devices: 79.4 us -> none  [per_device(): lax.psum_scatter(over_tokens(whole_values, branch_upstream), 'fs', scatte...]
    ppermute x0 -> x39, starting transfers between devices: none -> 52.1 us  [the longest x18 18.7 us: spread_rows(): lax.ppermute(block, axis, xor_pairs(size, bit))]
    psum x1 -> x0, blocking collectives: 39.3 us -> none  [per_device(): total = lax.psum(local_squares, ('fs', 'tp'))]
    dynamic_update_slice x0 -> x24, local copies, waits for them, and re-layouts: none -> 23.6 us  [the longest x21 23.5 us: spread_rows(): lax.dynamic_update_slice_in_dim(out, block, (spot ^ mark) * rows + part *...]
    dot_general x9 -> x8, matrix products: 33.4 us -> 10.7 us  [the longest x2 4.8 us: step_of(): jnp.dot(jnp.concatenate([basis, basis], axis=1), jnp.concatenate(two_term...]
  transfers between devices with their start and end apart: 7 -> 39, of which waited for: 7 -> 18; matrix products, arithmetic and copies ran while one was open for 3% -> 25% of each run, Pallas kernels for 0% -> 0%
where the time goes in v1:
time: 201 us; the launch traced here: 200 us
  waiting for transfers between devices  83.5 us (42%)
  starting transfers between devices  52.1 us (26%)
  local copies, waits for them, and re-layouts  41.6 us (21%)
  matrix products  10.7 us (5%)
  other arithmetic  7.64 us (4%)
  between operations  3.97 us (2%)
    ppermute x18, waiting for transfers between devices, spread_rows(): lax.ppermute(block, axis, xor_pairs(size, bit))  40.1 us
    dynamic_update_slice x21, local copies, waits for them, and re-layouts, spread_rows(): lax.dynamic_update_slice_in_dim(out, block, (spot ^ mark) * rows + part *...  23.5 us
    ppermute x18, starting transfers between devices, spread_rows(): lax.ppermute(block, axis, xor_pairs(size, bit))  18.7 us
    ppermute x3, waiting for transfers between devices, sum_over(): lax.ppermute(piece(half, (own_group + step) % groups, groups), axis, shif...  16 us
    ppermute x9, starting transfers between devices, doubling_sum(): lax.ppermute(value, axis, xor_pairs(size, order[stage]))  14.1 us
    ppermute x9, waiting for transfers between devices, doubling_sum(): lax.ppermute(value, axis, xor_pairs(size, order[stage]))  12.2 us
    ppermute x3, waiting for transfers between devices, sum_over(): lax.ppermute(total, axis, shift_pairs(groups, inner, step))  10.7 us
    unnamed x36, local copies, waits for them, and re-layouts  6.93 us
  transfers between devices with their start and end apart: 39, of which 18 were waited for; matrix products, arithmetic and copies ran while one was open for 25% of the time, Pallas kernels for 0%

profile of v1, /device:TPU:0, one launch (start us, length us, event | category | flops | bytes accessed | tf_op | source)
XLA Modules:
  0.0 199.5 jit_solution(14419359282660936679)
XLA Ops:
  5.5 2.0 %collective-permute-done = f32[512,384]{0,1:T(8,128)} collective-permute-done((f32[512,384]{0,1:T(8,128)S(1)}, f32[512,384]{0,1:T(8,128)}, u32[]{:S(2)}, u32[]{:S(2)}) %collective-permute-start) | collective-permute-done | bytes 786464 | tf_op jit(solution)/shard_map/ppermute | solution.py:63
  8.9 5.0 %collective-permute-start.3 = (f32[128,384]{0,1:T(8,128)S(1)}, f32[128,384]{0,1:T(8,128)S(1)}, u32[]{:S(2)}, u32[]{:S(2)}) collective-permute-start(f32[128,384]{0,1:T(8,128)S(1)} %get-tuple-element.68), channel_id=1, source_target_pairs={{0,6},{1,7},{2,0},{3,1},{4,2},{5,3},{6,4},{7,5},{8,14},{9,15},{10,... | collective-permute-start | bytes 589832 | tf_op jit(solution)/shard_map/ppermute | solution.py:66
  15.0 4.4 %collective-permute-done.3 = f32[128,384]{0,1:T(8,128)S(1)} collective-permute-done((f32[128,384]{0,1:T(8,128)S(1)}, f32[128,384]{0,1:T(8,128)S(1)}, u32[]{:S(2)}, u32[]{:S(2)}) %collective-permute-start.3) | collective-permute-done | bytes 196640 | tf_op jit(solution)/shard_map/ppermute | solution.py:66
  19.3 11.6 %collective-permute-done.2 = f32[128,384]{0,1:T(8,128)S(1)} collective-permute-done((f32[128,384]{0,1:T(8,128)S(1)}, f32[128,384]{0,1:T(8,128)S(1)}, u32[]{:S(2)}, u32[]{:S(2)}) %collective-permute-start.2) | collective-permute-done | bytes 196640 | tf_op jit(solution)/shard_map/ppermute | solution.py:66
  34.0 2.8 %collective-permute-start.6 = (f32[128,384]{0,1:T(8,128)S(1)}, f32[128,384]{0,1:T(8,128)S(1)}, u32[]{:S(2)}, u32[]{:S(2)}) collective-permute-start(f32[128,384]{0,1:T(8,128)S(1)} %get-tuple-element.52), channel_id=1, source_target_pairs={{0,6},{1,7},{2,0},{3,1},{4,2},{5,3},{6,4},{7,5},{8,14},{9,15},{10,... | collective-permute-start | bytes 589832 | tf_op jit(solution)/shard_map/ppermute | solution.py:75
  36.9 3.9 %collective-permute-done.4 = f32[128,384]{0,1:T(8,128)S(1)} collective-permute-done((f32[128,384]{0,1:T(8,128)S(1)}, f32[128,384]{0,1:T(8,128)S(1)}, u32[]{:S(2)}, u32[]{:S(2)}) %collective-permute-start.4) | collective-permute-done | bytes 196640 | tf_op jit(solution)/shard_map/ppermute | solution.py:75
  40.8 6.8 %collective-permute-done.5 = f32[128,384]{0,1:T(8,128)S(1)} collective-permute-done((f32[128,384]{0,1:T(8,128)S(1)}, f32[128,384]{0,1:T(8,128)S(1)}, u32[]{:S(2)}, u32[]{:S(2)}) %collective-permute-start.5) | collective-permute-done | bytes 196640 | tf_op jit(solution)/shard_map/ppermute | solution.py:75
  47.8 2.2 %collective-permute-done.7 = f32[512,384]{0,1:T(8,128)S(1)} collective-permute-done((f32[512,384]{0,1:T(8,128)S(1)}, f32[512,384]{0,1:T(8,128)S(1)}, u32[]{:S(2)}, u32[]{:S(2)}) %collective-permute-start.7) | collective-permute-done | bytes 786464 | tf_op jit(solution)/shard_map/ppermute | solution.py:82
  55.6 5.3 %collective-permute-done.10 = f32[128,128]{1,0:T(8,128)S(1)} collective-permute-done((f32[128,128]{1,0:T(8,128)S(1)}, f32[128,128]{1,0:T(8,128)S(1)}, u32[]{:S(2)}, u32[]{:S(2)}) %collective-permute-start.10) | collective-permute-done | bytes 65568 | tf_op jit(solution)/shard_map/ppermute | solution.py:104
  66.5 4.0 %collective-permute-done.9 = f32[128,512]{1,0:T(8,128)S(1)} collective-permute-done((f32[128,512]{1,0:T(8,128)S(1)}, f32[128,512]{1,0:T(8,128)S(1)}, u32[]{:S(2)}, u32[]{:S(2)}) %collective-permute-start.9) | collective-permute-done | bytes 262176 | tf_op jit(solution)/shard_map/ppermute | solution.py:104
  75.7 4.3 %collective-permute-start.15 = (f32[8,128]{1,0:T(8,128)S(1)}, f32[8,128]{1,0:T(8,128)S(1)}, u32[]{:S(2)}, u32[]{:S(2)}) collective-permute-start(f32[8,128]{1,0:T(8,128)S(1)} %broadcast_add_fusion), channel_id=1, source_target_pairs={{0,2},{1,3},{2,0},{3,1},{4,6},{5,7},{6,4},{7,5},{8,10},{9,11},{10,... | collective-permute-start | bytes 12296 | tf_op jit(solution)/shard_map/ppermute | solution.py:104
  81.6 2.2 %collective-permute-start.16 = (f32[8,128]{1,0:T(8,128)S(1)}, f32[8,128]{1,0:T(8,128)S(1)}, u32[]{:S(2)}, u32[]{:S(2)}) collective-permute-start(f32[8,128]{1,0:T(8,128)S(1)} %fusion.71), channel_id=1, source_target_pairs={{0,4},{1,5},{2,6},{3,7},{4,0},{5,1},{6,2},{7,3},{8,12},{9,13},{10,... | collective-permute-start | bytes 12296 | tf_op jit(solution)/shard_map/ppermute | solution.py:104
  86.4 4.2 %collective-permute-start.17 = (f32[512,128]{0,1:T(8,128)}, f32[512,128]{0,1:T(8,128)S(1)}, u32[]{:S(2)}, u32[]{:S(2)}) collective-permute-start(f32[512,128]{0,1:T(8,128)} %get-tuple-element.46), channel_id=1, source_target_pairs={{0,6},{1,7},{10,8},{11,9},{20,18},{21,19},{30,28},{31,29}} | collective-permute-start | bytes 786440 | tf_op jit(solution)/shard_map/ppermute | solution.py:156
  95.5 2.3 %fusion.57 = (bf16[1024,128]{1,0:T(8,128)(2,1)S(1)}, f32[1024,128]{1,0:T(8,128)}, f32[1024,128]{1,0:T(8,128)}) fusion(f32[1024,128]{1,0:T(8,128)} %param.23, bf16[128,128]{1,0:T(8,128)(2,1)S(1)} %fusion.44, bf16[128,128]{1,0:T(8,128)(2,1)S(1)} %get-tuple-element.39, bf16[1024,128]{1,0:T(8,128)(2,1)S(1)} %constant_dynamic-slice_fusion), kind=kOutput, calls=%fused_computation.143 | convolution fusion | flops 68681728 | bytes 2162688 | tf_op jit(solution)/shard_map/dot_general | solution.py:253
  100.6 2.5 %fusion.58 = (bf16[1024,512]{1,0:T(8,128)(2,1)S(1)}, f32[1024,512]{1,0:T(8,128)}, f32[1024,512]{1,0:T(8,128)}) fusion(f32[1024,512]{1,0:T(8,128)S(1)} %copy-done.4, bf16[128,512]{1,0:T(8,128)(2,1)S(1)} %fusion.33, bf16[128,512]{1,0:T(8,128)(2,1)S(1)} %get-tuple-element.42, bf16[1024,128]{1,0:T(8,128)(2,1)S(1)} %constant_dynamic-slice_fusion.7), kind=kOutput, calls=%fused_computation.144 | convolution fusion | flops 271581184 | bytes 7864320 | tf_op jit(solution)/shard_map/dot_general | solution.py:253
  111.7 2.3 %collective-permute-start.31 = (bf16[512,128]{1,0:T(8,128)(2,1)S(1)}, bf16[512,128]{1,0:T(8,128)(2,1)S(1)}, u32[]{:S(2)}, u32[]{:S(2)}) collective-permute-start(bf16[512,128]{1,0:T(8,128)(2,1)S(1)} %get-tuple-element.72), channel_id=1, source_target_pairs={{0,8},{8,0},{16,24},{24,16},{1,9},{9,1},{17,25},{25,17},{2,10},{10... | collective-permute-start | bytes 393224 | tf_op jit(solution)/shard_map/ppermute | solution.py:124
  115.2 8.5 %collective-permute-done.29 = bf16[512,128]{1,0:T(8,128)(2,1)S(1)} collective-permute-done((bf16[512,128]{1,0:T(8,128)(2,1)S(1)}, bf16[512,128]{1,0:T(8,128)(2,1)S(1)}, u32[]{:S(2)}, u32[]{:S(2)}) %collective-permute-start.29) | collective-permute-done | bytes 131104 | tf_op jit(solution)/shard_map/ppermute | solution.py:124
  126.6 2.6 %fusion.56 = (bf16[1024,512]{1,0:T(8,128)(2,1)S(1)}, f32[1024,512]{1,0:T(8,128)}, f32[1024,512]{1,0:T(8,128)}) fusion(f32[1024,512]{1,0:T(8,128)S(1)} %copy-done.5, bf16[512,128]{1,0:T(8,128)(2,1)S(1)} %get-tuple-element.78, bf16[1024,128]{0,1:T(8,128)(2,1)S(1)} %fusion.6, bf16[1024,128]{0,1:T(8,128)(2,1)S(1)} %get-tuple-element.36), kind=kOutput, calls=%fused_computation.142 | convolution fusion | flops 271581184 | bytes 7995392 | tf_op jit(solution)/shard_map/dot_general | solution.py:243
  129.2 2.3 %broadcast.17.clone.1 = bf16[4096,512]{1,0:T(8,128)(2,1)} broadcast(bf16[]{:T(256)} %constant.145.clone.1), dimensions={} | broadcast | bytes 4194306 | tf_op jit(solution)/shard_map/broadcast.2
  140.5 2.0 %copy.34 = f32[1024,128]{1,0:T(8,128)} copy(f32[1024,128]{0,1:T(8,128)} %copy-done.2) | data formatting | bytes 1048576
  152.2 9.2 %collective-permute-done.34 = bf16[512,512]{1,0:T(8,128)(2,1)} collective-permute-done((bf16[512,512]{1,0:T(8,128)(2,1)}, bf16[512,512]{1,0:T(8,128)(2,1)}, u32[]{:S(2)}, u32[]{:S(2)}) %collective-permute-start.34) | collective-permute-done | bytes 524320 | tf_op jit(solution)/shard_map/ppermute | solution.py:124
  163.6 9.0 %collective-permute-done.36 = bf16[512,512]{1,0:T(8,128)(2,1)} collective-permute-done((bf16[512,512]{1,0:T(8,128)(2,1)}, bf16[512,512]{1,0:T(8,128)(2,1)}, u32[]{:S(2)}, u32[]{:S(2)}) %collective-permute-start.36) | collective-permute-done | bytes 524320 | tf_op jit(solution)/shard_map/ppermute | solution.py:124
  174.7 9.2 %collective-permute-done.23 = bf16[512,512]{1,0:T(8,128)(2,1)} collective-permute-done((bf16[512,512]{1,0:T(8,128)(2,1)}, bf16[512,512]{1,0:T(8,128)(2,1)}, u32[]{:S(2)}, u32[]{:S(2)}) %collective-permute-start.23) | collective-permute-done | bytes 524320 | tf_op jit(solution)/shard_map/ppermute | solution.py:124
  190.5 3.9 %collective-permute-done.35 = bf16[512,512]{1,0:T(8,128)(2,1)S(1)} collective-permute-done((bf16[512,512]{1,0:T(8,128)(2,1)}, bf16[512,512]{1,0:T(8,128)(2,1)S(1)}, u32[]{:S(2)}, u32[]{:S(2)}) %collective-permute-start.35) | collective-permute-done | bytes 524320 | tf_op jit(solution)/shard_map/ppermute | solution.py:124
  (161 shorter events, 82.9 us)
Async XLA Ops:
  8.9 10.4 %collective-permute-start.3 = (f32[128,384]{0,1:T(8,128)S(1)}, f32[128,384]{0,1:T(8,128)S(1)}, u32[]{:S(2)}, u32[]{:S(2)}) collective-permute-start(f32[128,384]{0,1:T(8,128)S(1)} %get-tuple-element.68), channel_id=1, source_target_pairs={{0,6},{1,7},{2,0},{3,1},{4,2},{5,3},{6,4},{7,5},{8,14},{9,15},{10,... | collective-permute-start | bytes 589832 | tf_op jit(solution)/shard_map/ppermute | solution.py:66
  14.0 17.0 %collective-permute-start.2 = (f32[128,384]{0,1:T(8,128)S(1)}, f32[128,384]{0,1:T(8,128)S(1)}, u32[]{:S(2)}, u32[]{:S(2)}) collective-permute-start(f32[128,384]{0,1:T(8,128)S(1)} %get-tuple-element.69), channel_id=1, source_target_pairs={{0,4},{1,5},{2,6},{3,7},{4,0},{5,1},{6,2},{7,3},{8,12},{9,13},{10,... | collective-permute-start | bytes 589832 | tf_op jit(solution)/shard_map/ppermute | solution.py:66
  14.0 17.0 %collective-permute-start.1 = (f32[128,384]{0,1:T(8,128)S(1)}, f32[128,384]{0,1:T(8,128)S(1)}, u32[]{:S(2)}, u32[]{:S(2)}) collective-permute-start(f32[128,384]{0,1:T(8,128)S(1)} %get-tuple-element.67), channel_id=1, source_target_pairs={{0,2},{1,3},{2,4},{3,5},{4,6},{5,7},{6,0},{7,1},{8,10},{9,11},{10,... | collective-permute-start | bytes 589832 | tf_op jit(solution)/shard_map/ppermute | solution.py:66
  32.0 15.6 %collective-permute-start.5 = (f32[128,384]{0,1:T(8,128)S(1)}, f32[128,384]{0,1:T(8,128)S(1)}, u32[]{:S(2)}, u32[]{:S(2)}) collective-permute-start(f32[128,384]{0,1:T(8,128)S(1)} %get-tuple-element.52), channel_id=1, source_target_pairs={{0,4},{1,5},{2,6},{3,7},{4,0},{5,1},{6,2},{7,3},{8,12},{9,13},{10,... | collective-permute-start | bytes 589832 | tf_op jit(solution)/shard_map/ppermute | solution.py:75
  34.0 13.6 %collective-permute-start.6 = (f32[128,384]{0,1:T(8,128)S(1)}, f32[128,384]{0,1:T(8,128)S(1)}, u32[]{:S(2)}, u32[]{:S(2)}) collective-permute-start(f32[128,384]{0,1:T(8,128)S(1)} %get-tuple-element.52), channel_id=1, source_target_pairs={{0,6},{1,7},{2,0},{3,1},{4,2},{5,3},{6,4},{7,5},{8,14},{9,15},{10,... | collective-permute-start | bytes 589832 | tf_op jit(solution)/shard_map/ppermute | solution.py:75
  51.0 11.4 %collective-permute-start.8 = (f32[128,512]{1,0:T(8,128)S(1)}, f32[128,512]{1,0:T(8,128)S(1)}, u32[]{:S(2)}, u32[]{:S(2)}) collective-permute-start(f32[128,512]{1,0:T(8,128)S(1)} %slice_add_fusion.1), channel_id=1, source_target_pairs={{0,8},{8,0},{16,24},{24,16},{1,9},{9,1},{17,25},{25,17},{2,10},{10... | collective-permute-start | bytes 786440 | tf_op jit(solution)/shard_map/ppermute | solution.py:104
  81.6 11.6 %collective-permute-start.16 = (f32[8,128]{1,0:T(8,128)S(1)}, f32[8,128]{1,0:T(8,128)S(1)}, u32[]{:S(2)}, u32[]{:S(2)}) collective-permute-start(f32[8,128]{1,0:T(8,128)S(1)} %fusion.71), channel_id=1, source_target_pairs={{0,4},{1,5},{2,6},{3,7},{4,0},{5,1},{6,2},{7,3},{8,12},{9,13},{10,... | collective-permute-start | bytes 12296 | tf_op jit(solution)/shard_map/ppermute | solution.py:104
  86.4 25.3 %collective-permute-start.17 = (f32[512,128]{0,1:T(8,128)}, f32[512,128]{0,1:T(8,128)S(1)}, u32[]{:S(2)}, u32[]{:S(2)}) collective-permute-start(f32[512,128]{0,1:T(8,128)} %get-tuple-element.46), channel_id=1, source_target_pairs={{0,6},{1,7},{10,8},{11,9},{20,18},{21,19},{30,28},{31,29}} | collective-permute-start | bytes 786440 | tf_op jit(solution)/shard_map/ppermute | solution.py:156
  90.6 23.4 %collective-permute-start.18 = (f32[512,128]{0,1:T(8,128)}, f32[512,128]{0,1:T(8,128)S(1)}, u32[]{:S(2)}, u32[]{:S(2)}) collective-permute-start(f32[512,128]{0,1:T(8,128)} %get-tuple-element.46), channel_id=1, source_target_pairs={{0,4},{1,5},{10,14},{11,15},{20,16},{21,17},{30,26},{31,27}} | collective-permute-start | bytes 786440 | tf_op jit(solution)/shard_map/ppermute | solution.py:156
  92.0 22.1 %collective-permute-start.19 = (f32[512,128]{0,1:T(8,128)}, f32[512,128]{0,1:T(8,128)S(1)}, u32[]{:S(2)}, u32[]{:S(2)}) collective-permute-start(f32[512,128]{0,1:T(8,128)} %get-tuple-element.46), channel_id=1, source_target_pairs={{0,2},{1,3},{10,12},{11,13},{20,22},{21,23},{30,24},{31,25}} | collective-permute-start | bytes 786440 | tf_op jit(solution)/shard_map/ppermute | solution.py:156
  107.0 30.8 %collective-permute-start.21 = (bf16[512,512]{1,0:T(8,128)(2,1)S(1)}, bf16[512,512]{1,0:T(8,128)(2,1)}, u32[]{:S(2)}, u32[]{:S(2)}) collective-permute-start(bf16[512,512]{1,0:T(8,128)(2,1)S(1)} %get-tuple-element.66), channel_id=1, source_target_pairs={{0,8},{8,0},{16,24},{24,16},{1,9},{9,1},{17,25},{25,17},{2,10},{10... | collective-permute-start | bytes 1572872 | tf_op jit(solution)/shard_map/ppermute | solution.py:124
  109.7 30.0 %collective-permute-start.22 = (bf16[512,512]{1,0:T(8,128)(2,1)S(1)}, bf16[512,512]{1,0:T(8,128)(2,1)}, u32[]{:S(2)}, u32[]{:S(2)}) collective-permute-start(bf16[512,512]{1,0:T(8,128)(2,1)S(1)} %get-tuple-element.66), channel_id=1, source_target_pairs={{0,16},{8,24},{16,0},{24,8},{1,17},{9,25},{17,1},{25,9},{2,18},{10... | collective-permute-start | bytes 1572872 | tf_op jit(solution)/shard_map/ppermute | solution.py:124
  111.7 23.4 %collective-permute-start.31 = (bf16[512,128]{1,0:T(8,128)(2,1)S(1)}, bf16[512,128]{1,0:T(8,128)(2,1)S(1)}, u32[]{:S(2)}, u32[]{:S(2)}) collective-permute-start(bf16[512,128]{1,0:T(8,128)(2,1)S(1)} %get-tuple-element.72), channel_id=1, source_target_pairs={{0,8},{8,0},{16,24},{24,16},{1,9},{9,1},{17,25},{25,17},{2,10},{10... | collective-permute-start | bytes 393224 | tf_op jit(solution)/shard_map/ppermute | solution.py:124
  114.0 23.0 %collective-permute-start.32 = (bf16[512,128]{1,0:T(8,128)(2,1)S(1)}, bf16[512,128]{1,0:T(8,128)(2,1)S(1)}, u32[]{:S(2)}, u32[]{:S(2)}) collective-permute-start(bf16[512,128]{1,0:T(8,128)(2,1)S(1)} %collective-permute-done.30), channel_id=1, source_target_pairs={{0,8},{8,0},{16,24},{24,16},{1,9},{9,1},{17,25},{25,17},{2,10},{10... | collective-permute-start | bytes 393224 | tf_op jit(solution)/shard_map/ppermute | solution.py:124
  132.7 15.6 %collective-permute-start.33 = (bf16[512,512]{1,0:T(8,128)(2,1)}, bf16[512,512]{1,0:T(8,128)(2,1)}, u32[]{:S(2)}, u32[]{:S(2)}) collective-permute-start(bf16[512,512]{1,0:T(8,128)(2,1)} %get-tuple-element.63), channel_id=1, source_target_pairs={{0,8},{8,0},{16,24},{24,16},{1,9},{9,1},{17,25},{25,17},{2,10},{10... | collective-permute-start | bytes 1572872 | tf_op jit(solution)/shard_map/ppermute | solution.py:124
  135.1 15.7 %collective-permute-start.24 = (bf16[512,512]{1,0:T(8,128)(2,1)}, bf16[512,512]{1,0:T(8,128)(2,1)}, u32[]{:S(2)}, u32[]{:S(2)}) collective-permute-start(bf16[512,512]{1,0:T(8,128)(2,1)} %get-tuple-element.64), channel_id=1, source_target_pairs={{0,16},{8,24},{16,0},{24,8},{1,17},{9,25},{17,1},{25,9},{2,18},{10... | collective-permute-start | bytes 1572872 | tf_op jit(solution)/shard_map/ppermute | solution.py:124
  137.1 24.3 %collective-permute-start.34 = (bf16[512,512]{1,0:T(8,128)(2,1)}, bf16[512,512]{1,0:T(8,128)(2,1)}, u32[]{:S(2)}, u32[]{:S(2)}) collective-permute-start(bf16[512,512]{1,0:T(8,128)(2,1)} %get-tuple-element.63), channel_id=1, source_target_pairs={{0,16},{8,24},{16,0},{24,8},{1,17},{9,25},{17,1},{25,9},{2,18},{10... | collective-permute-start | bytes 1572872 | tf_op jit(solution)/shard_map/ppermute | solution.py:124
  137.8 34.8 %collective-permute-start.36 = (bf16[512,512]{1,0:T(8,128)(2,1)}, bf16[512,512]{1,0:T(8,128)(2,1)}, u32[]{:S(2)}, u32[]{:S(2)}) collective-permute-start(bf16[512,512]{1,0:T(8,128)(2,1)} %get-tuple-element.61), channel_id=1, source_target_pairs={{0,16},{8,24},{16,0},{24,8},{1,17},{9,25},{17,1},{25,9},{2,18},{10... | collective-permute-start | bytes 1572872 | tf_op jit(solution)/shard_map/ppermute | solution.py:124
  139.8 44.1 %collective-permute-start.23 = (bf16[512,512]{1,0:T(8,128)(2,1)}, bf16[512,512]{1,0:T(8,128)(2,1)}, u32[]{:S(2)}, u32[]{:S(2)}) collective-permute-start(bf16[512,512]{1,0:T(8,128)(2,1)} %collective-permute-done.21), channel_id=1, source_target_pairs={{0,16},{8,24},{16,0},{24,8},{1,17},{9,25},{17,1},{25,9},{2,18},{10... | collective-permute-start | bytes 1572872 | tf_op jit(solution)/shard_map/ppermute | solution.py:124
  148.3 40.5 %collective-permute-start.25 = (bf16[512,512]{1,0:T(8,128)(2,1)}, bf16[512,512]{1,0:T(8,128)(2,1)S(1)}, u32[]{:S(2)}, u32[]{:S(2)}) collective-permute-start(bf16[512,512]{1,0:T(8,128)(2,1)} %get-tuple-element.64), channel_id=1, source_target_pairs={{0,8},{8,0},{16,24},{24,16},{1,9},{9,1},{17,25},{25,17},{2,10},{10... | collective-permute-start | bytes 1572872 | tf_op jit(solution)/shard_map/ppermute | solution.py:124
  150.7 47.2 %collective-permute-start.37 = (bf16[512,512]{1,0:T(8,128)(2,1)}, bf16[512,512]{1,0:T(8,128)(2,1)S(1)}, u32[]{:S(2)}, u32[]{:S(2)}) collective-permute-start(bf16[512,512]{1,0:T(8,128)(2,1)} %get-tuple-element.61), channel_id=1, source_target_pairs={{0,8},{8,0},{16,24},{24,16},{1,9},{9,1},{17,25},{25,17},{2,10},{10... | collective-permute-start | bytes 1572872 | tf_op jit(solution)/shard_map/ppermute | solution.py:124
  161.4 28.2 %collective-permute-start.26 = (bf16[512,512]{1,0:T(8,128)(2,1)}, bf16[512,512]{1,0:T(8,128)(2,1)S(1)}, u32[]{:S(2)}, u32[]{:S(2)}) collective-permute-start(bf16[512,512]{1,0:T(8,128)(2,1)} %collective-permute-done.24), channel_id=1, source_target_pairs={{0,8},{8,0},{16,24},{24,16},{1,9},{9,1},{17,25},{25,17},{2,10},{10... | collective-permute-start | bytes 1572872 | tf_op jit(solution)/shard_map/ppermute | solution.py:124
  172.7 21.7 %collective-permute-start.35 = (bf16[512,512]{1,0:T(8,128)(2,1)}, bf16[512,512]{1,0:T(8,128)(2,1)S(1)}, u32[]{:S(2)}, u32[]{:S(2)}) collective-permute-start(bf16[512,512]{1,0:T(8,128)(2,1)} %collective-permute-done.33), channel_id=1, source_target_pairs={{0,16},{8,24},{16,0},{24,8},{1,17},{9,25},{17,1},{25,9},{2,18},{10... | collective-permute-start | bytes 1572872 | tf_op jit(solution)/shard_map/ppermute | solution.py:124
  183.9 14.8 %collective-permute-start.38 = (bf16[512,512]{1,0:T(8,128)(2,1)}, bf16[512,512]{1,0:T(8,128)(2,1)S(1)}, u32[]{:S(2)}, u32[]{:S(2)}) collective-permute-start(bf16[512,512]{1,0:T(8,128)(2,1)} %collective-permute-done.36), channel_id=1, source_target_pairs={{0,8},{8,0},{16,24},{24,16},{1,9},{9,1},{17,25},{25,17},{2,10},{10... | collective-permute-start | bytes 1572872 | tf_op jit(solution)/shard_map/ppermute | solution.py:124
  (31 other events, 250.7 us)
